TPU v7x, 32 devices: a whole 2x2x4 slice. The times are simulated.
32 devices in a mesh: ep: 8 (over z, core), tp: 4 (over y, x).
Axes of the slice: x: 2, y: 2, z: 4, core: 2. Of those that a mesh axis runs over, the one named last changes fastest.
Arguments:
- tokens: bfloat16 [64, 2048], P('ep'), may hold values from -6 to 6
- attn_gain: float32 [2048], replicated, may hold values from 0.1 to 1.9
- query_weight: bfloat16 [2048, 4096], P('ep', 'tp'), may hold values from -0.125 to 0.125
- key_weight: bfloat16 [2048, 4096], P('ep', 'tp'), may hold values from -0.125 to 0.125
- value_weight: bfloat16 [2048, 4096], P('ep', 'tp'), may hold values from -0.125 to 0.125
- query_gain: float32 [128], replicated, may hold values from 0.1 to 1.9
- stick_bias: float32 [32], P('tp'), may hold values from -7 to -2.5
- key_cache: bfloat16 [64, 32, 512, 128], P('ep', 'tp'), may hold values from -6 to 6
- value_cache: bfloat16 [64, 32, 512, 128], P('ep', 'tp'), may hold values from -6 to 6
- lengths: int32 [64], P('ep'), may hold values from 64 to 512, as said below
- out_weight: bfloat16 [4096, 2048], P('tp'), may hold values from -0.375 to 0.375
- mix_gain: float32 [2048], replicated, may hold values from 0.1 to 1.9
- route_ids: int32 [64, 2], P('ep'), may hold values from 0 to 7, all different within a row; in each aligned block of 8 rows (0 to 7, 8 to 15, ...) at most 4 rows name the same one
- route_weights: float32 [64, 2], P('ep'), may hold values from 0.2 to 1
- expert_gate: bfloat16 [8, 2048, 2560], P('ep', None, 'tp'), may hold values from -0.125 to 0.125
- expert_up: bfloat16 [8, 2048, 2560], P('ep', None, 'tp'), may hold values from -0.125 to 0.125
- expert_down: bfloat16 [8, 2560, 2048], P('ep', 'tp'), may hold values from -0.15625 to 0.15625
- side_gate: bfloat16 [2048, 1024], P(None, 'tp'), may hold values from -0.125 to 0.125
- side_up: bfloat16 [2048, 1024], P(None, 'tp'), may hold values from -0.125 to 0.125
- side_down: bfloat16 [1024, 2048], P('tp'), may hold values from -0.25 to 0.25
- branch_gate: float32 [2048], replicated, may hold values from -0.125 to 0.125
Outputs:
- mixed: bfloat16 [64, 2048], P('ep', 'tp')
- new_keys: bfloat16 [64, 4096], P('ep', 'tp')
- new_values: bfloat16 [64, 4096], P('ep', 'tp')
Inputs may be any that keep to these rules, and one draw needn't show every extreme that they name: `lengths`: at least an eighth of 512; the first sequence has 512. `route_ids`: each token names 2 different experts. In the rows of one device no expert is named by more than 4 rows, a bound that some block reaches of some device.
All inputs are finite; a program needn't handle non-finite values.
Results may differ from a plain program's by a relative error of at most 0.018.
Values may be sent and summed in bfloat16 or wider, within the bound.
No kernel may reach another device: no remote copies, remote signals or barrier semaphores. Data moves between devices by JAX's collectives and lax.ppermute only.
A program may use at most 64 MiB of HBM per device.

v0:
```python
import jax
import jax.numpy as jnp
from jax import lax
from jax.sharding import PartitionSpec as P

DH = 128
epsilon = 1e-06


def rms_scale(values, scale_gain):
    mean_square = jnp.mean(values * values, axis=-1, keepdims=True)
    return values * lax.rsqrt(mean_square + epsilon) * scale_gain


def body(
    tokens,
    attn_gain,
    query_weight,
    key_weight,
    value_weight,
    query_gain,
    stick_bias,
    key_cache,
    value_cache,
    lengths,
    out_weight,
    mix_gain,
    route_ids,
    route_weights,
    expert_gate,
    expert_up,
    expert_down,
    side_gate,
    side_up,
    side_down,
    branch_gate,
):
    seq_count, model_width = tokens.shape
    head_cols = query_weight.shape[1]
    heads_local = key_cache.shape[1]
    cache_slots = key_cache.shape[2]
    stream = tokens.astype(jnp.float32)
    normed = rms_scale(stream, attn_gain).astype(jnp.bfloat16)
    stacked = jnp.concatenate([query_weight, key_weight, value_weight], axis=1)
    columns = lax.all_to_all(normed, "ep", split_axis=1, concat_axis=0, tiled=True)
    picked = columns
    projected = lax.psum_scatter(
        jnp.dot(picked, stacked, preferred_element_type=jnp.float32),
        "ep",
        scatter_dimension=0,
        tiled=True,
    )
    query_rows = projected[:, :head_cols].astype(jnp.bfloat16)
    fresh_keys = projected[:, head_cols : 2 * head_cols].astype(jnp.bfloat16)
    new_values = projected[:, 2 * head_cols :].astype(jnp.bfloat16)
    new_keys = rms_scale(fresh_keys.astype(jnp.float32).reshape(seq_count, heads_local, DH), 1.0)
    new_keys = new_keys.astype(jnp.bfloat16).reshape(seq_count, head_cols)
    query_heads = rms_scale(
        query_rows.astype(jnp.float32).reshape(seq_count, heads_local, DH), query_gain
    )
    query_heads = query_heads.astype(jnp.bfloat16)
    scores = jnp.einsum("shd,shld->shl", query_heads, key_cache, preferred_element_type=jnp.float32)
    scores = scores * DH ** (-0.5) + stick_bias[None, :, None]
    positions = jnp.arange(cache_slots, dtype=jnp.int32)
    visible = positions[None, None, :] < lengths[:, None, None]
    log_rest = jnp.where(visible, jax.nn.log_sigmoid(-scores), 0.0)
    log_between = lax.cumsum(log_rest, axis=2, reverse=True) - log_rest
    stick = jnp.where(visible, jnp.exp(jax.nn.log_sigmoid(scores) + log_between), 0.0).astype(
        jnp.bfloat16
    )
    attended = jnp.einsum("shl,shld->shd", stick, value_cache, preferred_element_type=jnp.float32)
    attended = attended.astype(jnp.bfloat16).reshape(seq_count, head_cols)
    attn_proj = lax.psum(
        jnp.dot(attended, out_weight, preferred_element_type=jnp.float32).astype(jnp.bfloat16), "tp"
    ).astype(jnp.float32)
    middle = (stream + attn_proj).astype(jnp.bfloat16)
    normed_mix = rms_scale(middle.astype(jnp.float32), mix_gain).astype(jnp.bfloat16)
    side_gate_pre = jnp.dot(normed_mix, side_gate, preferred_element_type=jnp.float32)
    side_up_pre = jnp.dot(normed_mix, side_up, preferred_element_type=jnp.float32)
    side_hidden = (jax.nn.silu(side_gate_pre) * side_up_pre).astype(jnp.bfloat16)
    side_term = jnp.dot(side_hidden, side_down, preferred_element_type=jnp.float32)
    switch = jax.nn.sigmoid(
        jnp.sum(normed_mix.astype(jnp.float32) * branch_gate, axis=1, keepdims=True)
    )
    experts = lax.axis_size("ep")
    top_count = route_ids.shape[1]
    capacity = max(2, 2 * top_count * seq_count // experts)
    flat_ids = route_ids.reshape(-1)
    onehot = (flat_ids[:, None] == jnp.arange(experts, dtype=jnp.int32)[None, :]).astype(jnp.int32)
    before = jnp.cumsum(onehot, axis=0) - onehot
    slot_index = jnp.sum(before * onehot, axis=1)
    target = flat_ids * capacity + slot_index
    route_map = (
        target[:, None] == jnp.arange(experts * capacity, dtype=jnp.int32)[None, :]
    ).astype(jnp.bfloat16)
    dispatch = jnp.sum(route_map.reshape(seq_count, top_count, experts * capacity), axis=1).T
    outbox = jnp.dot(dispatch, normed_mix, preferred_element_type=jnp.float32).astype(jnp.bfloat16)
    outbox = outbox.reshape(experts, capacity, model_width)
    col_width = model_width // lax.axis_size("tp")
    col_offset = lax.axis_index("tp") * col_width
    arrived = lax.all_to_all(outbox, "ep", split_axis=0, concat_axis=0, tiled=True)
    slot_rows = arrived.reshape(experts * capacity, model_width)
    gate_pre = jnp.dot(slot_rows, expert_gate[0], preferred_element_type=jnp.float32)
    up_pre = jnp.dot(slot_rows, expert_up[0], preferred_element_type=jnp.float32)
    hidden = (jax.nn.silu(gate_pre) * up_pre).astype(jnp.bfloat16)
    expert_term = jnp.dot(hidden, expert_down[0], preferred_element_type=jnp.float32)
    expert_part, side_part = (
        lax.psum_scatter(
            expert_term.astype(jnp.bfloat16), "tp", scatter_dimension=1, tiled=True
        ).astype(jnp.float32),
        lax.psum_scatter(
            side_term.astype(jnp.bfloat16), "tp", scatter_dimension=1, tiled=True
        ).astype(jnp.float32),
    )
    returned = lax.all_to_all(
        expert_part.astype(jnp.bfloat16).reshape(experts, capacity, col_width),
        "ep",
        split_axis=0,
        concat_axis=0,
        tiled=True,
    )
    picked = jnp.dot(
        route_map,
        returned.reshape(experts * capacity, col_width),
        preferred_element_type=jnp.float32,
    )
    routed = jnp.sum(
        route_weights[:, :, None] * picked.reshape(seq_count, top_count, col_width), axis=1
    )
    middle_cols = lax.dynamic_slice_in_dim(middle, col_offset, col_width, 1).astype(jnp.float32)
    mixed = (middle_cols + routed + switch * side_part).astype(jnp.bfloat16)
    return (mixed, new_keys, new_values)


def solution(mesh):
    in_specs = (
        P("ep", None),
        P(),
        P("ep", "tp"),
        P("ep", "tp"),
        P("ep", "tp"),
        P(),
        P("tp"),
        P("ep", "tp", None, None),
        P("ep", "tp", None, None),
        P("ep"),
        P("tp", None),
        P(),
        P("ep", None),
        P("ep", None),
        P("ep", None, "tp"),
        P("ep", None, "tp"),
        P("ep", "tp", None),
        P(None, "tp"),
        P(None, "tp"),
        P("tp", None),
        P(),
    )
    out_specs = (P("ep", "tp"), P("ep", "tp"), P("ep", "tp"))
    return jax.shard_map(body, mesh=mesh, in_specs=in_specs, out_specs=out_specs, check_vma=False)
```

profile of v0, /device:TPU:0, one launch (start us, length us, event | category | flops | bytes accessed | tf_op | source)
XLA Modules:
  0.0 196.1 jit_solution(3717251648128114793)
XLA Ops:
  7.3 1.0 fusion.44
  8.3 0.8 fusion.46
  9.1 11.9 %all_to_all.29 = bf16[8,8,256]{2,0,1:T(8,128)(2,1)S(1)} all-to-all(bf16[8,8,256]{2,0,1:T(8,128)(2,1)S(1)} %bitcast.88), channel_id=1, replica_groups=mesh['ep'=8,'tp'=4] {'ep'}, dimensions={1} | all-to-all | bytes 65536 | tf_op jit(solution)/shard_map/all_to_all | solution.py:45
  21.0 2.6 %fusion.9 = f32[64,3072]{1,0:T(8,128)} fusion(bf16[256,1024]{1,0:T(8,128)(2,1)} %param.25, bf16[256,1024]{1,0:T(8,128)(2,1)} %param.24, bf16[256,1024]{1,0:T(8,128)(2,1)} %param.23, bf16[8,8,256]{2,0,1:T(8,128)(2,1)S(1)} %all_to_all.29), kind=kOutput, calls=%fused_computation.10 | convolution fusion | flops 105381888 | bytes 2392064 | tf_op jit(solution)/shard_map/dot_general | solution.py:48
  24.5 29.5 %reduce-scatter.4.cloned.1.call-done = f32[8,3072]{1,0:T(8,128)} async-done(((f32[64,3072]{1,0:T(8,128)}), f32[8,3072]{1,0:T(8,128)}) %reduce-scatter.4.cloned.1.call-update) | async-done | bytes 98320 | tf_op jit(solution)/shard_map/reduce_scatter | solution.py:47
  54.0 0.9 convert.7
  55.1 5.7 %fusion.57 = f32[8,8,1,512]{3,2,1,0:T(1,128)S(1)} fusion(bf16[8,8,512,128]{3,2,1,0:T(8,128)(2,1)} %param.28, bf16[8,8,128,1]{2,0,1,3:T(8,128)(2,1)S(1)} %fusion.59), kind=kOutput, calls=%fused_computation.68 | convolution fusion | flops 8388608 | bytes 8536064 | tf_op jit(solution)/shard_map/shd,shld->shl/dot_general | solution.py:62
  61.0 39.6 %reduce-window.6 = f32[8,8,4,128]{3,1,2,0:T(8,128)S(1)} reduce-window(f32[8,8,4,128]{3,1,2,0:T(8,128)S(1)} %fusion.35, f32[]{:T(128)} %constant.17.clone.1), window={size=1x1x1x128 pad=0_0x0_0x0_0x0_127}, to_apply=%region_3.0 | reduce-window | flops 4161536 | bytes 262148 | tf_op jit(solution)/shard_map/reduce-window
  101.3 4.7 %fusion.33 = f32[8,8,1,128]{3,2,1,0:T(1,128)S(1)} fusion(bf16[8,8,512,128]{3,2,1,0:T(8,128)(2,1)} %param.29, bf16[8,8,512,1]{2,1,0,3:T(8,128)(2,1)S(1)} %fusion.48), kind=kOutput, calls=%fused_computation.34 | convolution fusion | flops 8388608 | bytes 8486912 | tf_op jit(solution)/shard_map/shl,shld->shd/dot_general | solution.py:71
  106.7 16.2 %psum.7 = bf16[8,2048]{1,0:T(8,128)(2,1)S(1)} all-reduce(bf16[8,2048]{1,0:T(8,128)(2,1)S(1)} %convolution_convert_fusion.2), channel_id=1, replica_groups=mesh['ep'=8,'tp'=4] {'tp'}, use_global_device_ids=true, to_apply=%region_5.6 | all-reduce | flops 16384 | bytes 65536 | tf_op jit(solution)/shard_map/psum | solution.py:73
  123.4 0.7 reshape.161
  124.1 3.4 %all-to-all-start.1 = ((bf16[8,4,2048]{2,1,0:T(4,128)(2,1)}), bf16[8,4,2048]{2,1,0:T(4,128)(2,1)S(1)}, u32[]{:S(2)}, u32[]{:S(2)}) async-start(bf16[8,4,2048]{2,1,0:T(4,128)(2,1)} %reshape.161), calls=%async_computation.2 | async-start | bytes 262144 | tf_op jit(solution)/shard_map/all_to_all | solution.py:101
  127.5 1.5 fusion.81
  129.8 0.7 fusion.52
  130.5 3.6 %all-to-all-done.1 = bf16[8,4,2048]{2,1,0:T(4,128)(2,1)S(1)} async-done(((bf16[8,4,2048]{2,1,0:T(4,128)(2,1)}), bf16[8,4,2048]{2,1,0:T(4,128)(2,1)S(1)}, u32[]{:S(2)}, u32[]{:S(2)}) %all-to-all-start.1) | async-done | bytes 131104 | tf_op jit(solution)/shard_map/all_to_all | solution.py:101
  134.2 2.3 %fusion.4 = f32[32,640]{1,0:T(8,128)S(1)} fusion(bf16[32,2048]{1,0:T(8,128)(2,1)S(1)} %reshape.162, bf16[1,2048,640]{2,1,0:T(8,128)(2,1)} %param.35), kind=kOutput, calls=%fused_computation.4 | convolution fusion | flops 83886080 | bytes 2834432 | tf_op jit(solution)/shard_map/dot_general | solution.py:103
  136.5 3.4 %fusion.6 = bf16[32,2048]{1,0:T(8,128)(2,1)} fusion(bf16[1,640,2048]{2,1,0:T(8,128)(2,1)S(1)} %copy-done, bf16[32,2048]{1,0:T(8,128)(2,1)S(1)} %reshape.162, bf16[1,2048,640]{2,1,0:T(8,128)(2,1)} %param.36, f32[32,640]{1,0:T(8,128)S(1)} %fusion.4), kind=kOutput, calls=%fused_computation.6 | convolution fusion | flops 167960576 | bytes 5586944 | tf_op jit(solution)/shard_map/dot_general | solution.py:106
  139.9 2.9 %convolution_convert_fusion.1 = bf16[8,2048]{1,0:T(8,128)(2,1)} fusion(bf16[256,2048]{1,0:T(8,128)(2,1)} %param.40, bf16[2048,256]{1,0:T(8,128)(2,1)} %param.39, f32[8,256]{1,0:T(8,128)S(1)} %fusion.81, bf16[8,2048]{1,0:T(8,128)(2,1)S(1)} %get-tuple-element.6, f32[2048]{0:T(1024)S(1)} %copy-done.3, f32[8]{0:T(128)S(1)} %add_rsqrt_fusion.2), kind=kOutput, calls=%fused_computation.8 | convolution fusion | flops 16871424 | bytes 2179104 | tf_op jit(solution)/shard_map/dot_general | solution.py:81
  142.8 18.5 %reduce-scatter.6.cloned.1.call-done = bf16[32,512]{1,0:T(8,128)(2,1)} async-done(((bf16[32,2048]{1,0:T(8,128)(2,1)}), bf16[32,512]{1,0:T(8,128)(2,1)}) %reduce-scatter.6.cloned.1.call-update) | async-done | bytes 32784 | tf_op jit(solution)/shard_map/reduce_scatter | solution.py:108
  161.4 1.4 reshape.163
  162.7 4.6 %all-to-all-start.2 = ((bf16[8,4,512]{2,1,0:T(4,128)(2,1)}), bf16[8,4,512]{2,1,0:T(4,128)(2,1)S(1)}, u32[]{:S(2)}, u32[]{:S(2)}) async-start(bf16[8,4,512]{2,1,0:T(4,128)(2,1)} %reshape.163), calls=%async_computation.4 | async-start | bytes 65536 | tf_op jit(solution)/shard_map/all_to_all | solution.py:115
  167.3 5.7 %all-to-all-done.2 = bf16[8,4,512]{2,1,0:T(4,128)(2,1)S(1)} async-done(((bf16[8,4,512]{2,1,0:T(4,128)(2,1)}), bf16[8,4,512]{2,1,0:T(4,128)(2,1)S(1)}, u32[]{:S(2)}, u32[]{:S(2)}) %all-to-all-start.2) | async-done | bytes 32800 | tf_op jit(solution)/shard_map/all_to_all | solution.py:115
  173.3 14.9 %reduce-scatter.8.cloned.1.call-done = bf16[8,512]{1,0:T(8,128)(2,1)} async-done(((bf16[8,2048]{1,0:T(8,128)(2,1)}), bf16[8,512]{1,0:T(8,128)(2,1)}) %reduce-scatter.8.cloned.1.call-update) | async-done | bytes 8208 | tf_op jit(solution)/shard_map/reduce_scatter | solution.py:111
  188.2 1.4 add_convert_fusion
  (58 shorter events, 4.1 us)
Async XLA Ops:
  7.2 129.3 %copy-start = (bf16[1,640,2048]{2,1,0:T(8,128)(2,1)S(1)}, bf16[1,640,2048]{2,1,0:T(8,128)(2,1)}, u32[]{:S(2)}) copy-start(bf16[1,640,2048]{2,1,0:T(8,128)(2,1)} %param.37) | copy-start | bytes 7864324
  7.2 16.5 %copy-start.6 = (s32[8,2]{0,1:T(2,128)S(1)}, s32[8,2]{0,1:T(2,128)}, u32[]{:S(2)}) copy-start(s32[8,2]{0,1:T(2,128)} %param.33) | copy-start | bytes 196
  7.2 17.2 %copy-start.8 = (s32[8]{0:T(128)S(1)}, s32[8]{0:T(128)}, u32[]{:S(2)}) copy-start(s32[8]{0:T(128)} %param.30) | copy-start | bytes 100
  7.2 47.8 %copy-start.7 = (f32[128]{0:T(128)S(1)}, f32[128]{0:T(128)}, u32[]{:S(2)}) copy-start(f32[128]{0:T(128)} %param.26) | copy-start | bytes 1540
  7.2 46.8 %reduce-scatter.4.cloned.1.call-start = ((), (), s32[]{:S(2)}) async-start(), calls=%async_computation.6 | async-start | bytes 884736 | tf_op jit(solution)/shard_map/reduce_scatter | solution.py:47
  55.1 5.7 %copy-start.5 = (f32[8]{0:T(128)S(1)}, f32[8]{0:T(128)}, u32[]{:S(2)}) copy-start(f32[8]{0:T(128)} %param.27) | copy-start | bytes 100
  101.3 4.8 %copy-start.1 = (bf16[1024,2048]{1,0:T(8,128)(2,1)S(1)}, bf16[1024,2048]{1,0:T(8,128)(2,1)}, u32[]{:S(2)}) copy-start(bf16[1024,2048]{1,0:T(8,128)(2,1)} %param.31) | copy-start | bytes 12582916
  106.0 17.0 %copy-start.2 = (bf16[8,2048]{1,0:T(8,128)(2,1)S(1)}, bf16[8,2048]{1,0:T(8,128)(2,1)}, u32[]{:S(2)}) copy-start(bf16[8,2048]{1,0:T(8,128)(2,1)} %param.21) | copy-start | bytes 98308
  106.0 17.1 %copy-start.3 = (f32[2048]{0:T(1024)S(1)}, f32[2048]{0:T(1024)}, u32[]{:S(2)}) copy-start(f32[2048]{0:T(1024)} %param.32) | copy-start | bytes 24580
  106.0 23.0 %copy-start.4 = (f32[2048]{0:T(1024)S(1)}, f32[2048]{0:T(1024)}, u32[]{:S(2)}) copy-start(f32[2048]{0:T(1024)} %param.41) | copy-start | bytes 24580
  124.1 10.1 %all-to-all-start.1 = ((bf16[8,4,2048]{2,1,0:T(4,128)(2,1)}), bf16[8,4,2048]{2,1,0:T(4,128)(2,1)S(1)}, u32[]{:S(2)}, u32[]{:S(2)}) async-start(bf16[8,4,2048]{2,1,0:T(4,128)(2,1)} %reshape.161), calls=%async_computation.2 | async-start | bytes 262144 | tf_op jit(solution)/shard_map/all_to_all | solution.py:101
  127.4 33.9 %reduce-scatter.6.cloned.1.call-start = ((), (), s32[]{:S(2)}) async-start(), calls=%async_computation.7 | async-start | bytes 163840 | tf_op jit(solution)/shard_map/reduce_scatter | solution.py:108
  136.4 36.7 %copy-start.9 = (f32[8,2]{0,1:T(2,128)S(1)}, f32[8,2]{0,1:T(2,128)}, u32[]{:S(2)}) copy-start(f32[8,2]{0,1:T(2,128)} %param.34) | copy-start | bytes 196
  139.9 48.3 %reduce-scatter.8.cloned.1.call-start = ((), (), s32[]{:S(2)}) async-start(), calls=%async_computation.8 | async-start | bytes 40960 | tf_op jit(solution)/shard_map/reduce_scatter | solution.py:111
  162.7 10.4 %all-to-all-start.2 = ((bf16[8,4,512]{2,1,0:T(4,128)(2,1)}), bf16[8,4,512]{2,1,0:T(4,128)(2,1)S(1)}, u32[]{:S(2)}, u32[]{:S(2)}) async-start(bf16[8,4,512]{2,1,0:T(4,128)(2,1)} %reshape.163), calls=%async_computation.4 | async-start | bytes 65536 | tf_op jit(solution)/shard_map/all_to_all | solution.py:115
Sparse Core Ops, SparseCore 0:
  23.8 30.1 reduce-scatter.3
  140.0 21.3 reduce-scatter.5
  164.1 24.0 reduce-scatter.7
where the time goes:
time: 197 us; the launch traced here: 196 us
  waiting for transfers between devices  72.3 us (37%)
  other arithmetic  46 us (23%)
  blocking collectives  28.1 us (14%)
  matrix products  24.1 us (12%)
  between operations  14 us (7%)
  starting transfers between devices  8.11 us (4%)
  local copies, waits for them, and re-layouts  3.37 us (2%)
    another operation x3, other arithmetic  40.6 us
    reduce_scatter x1, waiting for transfers between devices, body(): lax.psum_scatter(jnp.dot(picked, stacked, preferred_element_type=jnp.floa...  29.5 us
    reduce_scatter x1, waiting for transfers between devices, body(): lax.psum_scatter(expert_term.astype(jnp.bfloat16), 'tp', scatter_dimensio...  18.5 us
    psum x1, blocking collectives, body(): lax.psum(jnp.dot(attended, out_weight, preferred_element_type=jnp.float32...  16.2 us
    reduce_scatter x1, waiting for transfers between devices, body(): lax.psum_scatter(side_term.astype(jnp.bfloat16), 'tp', scatter_dimension=...  14.9 us
    all_to_all x1, blocking collectives, body(): lax.all_to_all(normed, 'ep', split_axis=1, concat_axis=0, tiled=True)  11.9 us
    all_to_all x1, waiting for transfers between devices, body(): lax.all_to_all(expert_part.astype(jnp.bfloat16).reshape(experts, capacity...  5.73 us
    dot_general x1, matrix products, body(): jnp.einsum('shd,shld->shl', query_heads, key_cache, preferred_element_typ...  5.65 us
  transfers between devices with their start and end apart: 5, of which 5 were waited for; matrix products, arithmetic and copies ran while one was open for 4% of the time, Pallas kernels for 0%

commit v1 on v0

--- a/solution.py
+++ b/solution.py
@@ -70,8 +70,12 @@
     )
     attended = jnp.einsum("shl,shld->shd", stick, value_cache, preferred_element_type=jnp.float32)
     attended = attended.astype(jnp.bfloat16).reshape(seq_count, head_cols)
-    attn_proj = lax.psum(
-        jnp.dot(attended, out_weight, preferred_element_type=jnp.float32).astype(jnp.bfloat16), "tp"
+    attn_proj = jnp.sum(
+        lax.all_gather(
+            jnp.dot(attended, out_weight, preferred_element_type=jnp.float32).astype(jnp.bfloat16),
+            "tp",
+        ),
+        axis=0,
     ).astype(jnp.float32)
     middle = (stream + attn_proj).astype(jnp.bfloat16)
     normed_mix = rms_scale(middle.astype(jnp.float32), mix_gain).astype(jnp.bfloat16)

time: 197 us -> 190 us (0.964)
  blocking collectives: 28.1 us -> 20.3 us
    psum x1 -> x0, blocking collectives: 16.2 us -> none  [body(): lax.psum(jnp.dot(attended, out_weight, preferred_element_type=jnp.float32...]
    all_gather x0 -> x1, blocking collectives: none -> 8.4 us  [body(): lax.all_gather(jnp.dot(attended, out_weight, preferred_element_type=jnp.f...]
where the time goes in v1:
time: 190 us; the launch traced here: 189 us
  waiting for transfers between devices  73.2 us (39%)
  other arithmetic  46 us (24%)
  matrix products  24.1 us (13%)
  blocking collectives  20.3 us (11%)
  between operations  14 us (7%)
  starting transfers between devices  8.11 us (4%)
  local copies, waits for them, and re-layouts  3.37 us (2%)
    another operation x3, other arithmetic  40.6 us
    reduce_scatter x1, waiting for transfers between devices, body(): lax.psum_scatter(jnp.dot(picked, stacked, preferred_element_type=jnp.floa...  29.5 us
    reduce_scatter x1, waiting for transfers between devices, body(): lax.psum_scatter(expert_term.astype(jnp.bfloat16), 'tp', scatter_dimensio...  19.4 us
    reduce_scatter x1, waiting for transfers between devices, body(): lax.psum_scatter(side_term.astype(jnp.bfloat16), 'tp', scatter_dimension=...  14.9 us
    all_to_all x1, blocking collectives, body(): lax.all_to_all(normed, 'ep', split_axis=1, concat_axis=0, tiled=True)  11.9 us
    all_gather x1, blocking collectives, body(): lax.all_gather(jnp.dot(attended, out_weight, preferred_element_type=jnp.f...  8.4 us
    all_to_all x1, waiting for transfers between devices, body(): lax.all_to_all(expert_part.astype(jnp.bfloat16).reshape(experts, capacity...  5.73 us
    dot_general x1, matrix products, body(): jnp.einsum('shd,shld->shl', query_heads, key_cache, preferred_element_typ...  5.65 us
  transfers between devices with their start and end apart: 5, of which 5 were waited for; matrix products, arithmetic and copies ran while one was open for 4% of the time, Pallas kernels for 0%

profile of v1, /device:TPU:0, one launch (start us, length us, event | category | flops | bytes accessed | tf_op | source)
XLA Modules:
  0.0 189.1 jit_solution(3508109347569747391)
XLA Ops:
  7.3 1.0 fusion.44
  8.3 0.8 fusion.46
  9.1 11.9 %all_to_all.29 = bf16[8,8,256]{2,0,1:T(8,128)(2,1)S(1)} all-to-all(bf16[8,8,256]{2,0,1:T(8,128)(2,1)S(1)} %bitcast.90), channel_id=1, replica_groups=mesh['ep'=8,'tp'=4] {'ep'}, dimensions={1} | all-to-all | bytes 65536 | tf_op jit(solution)/shard_map/all_to_all | solution.py:45
  21.0 2.6 %fusion.9 = f32[64,3072]{1,0:T(8,128)} fusion(bf16[256,1024]{1,0:T(8,128)(2,1)} %param.25, bf16[256,1024]{1,0:T(8,128)(2,1)} %param.24, bf16[256,1024]{1,0:T(8,128)(2,1)} %param.23, bf16[8,8,256]{2,0,1:T(8,128)(2,1)S(1)} %all_to_all.29), kind=kOutput, calls=%fused_computation.10 | convolution fusion | flops 105381888 | bytes 2392064 | tf_op jit(solution)/shard_map/dot_general | solution.py:48
  24.5 29.5 %reduce-scatter.4.cloned.1.call-done = f32[8,3072]{1,0:T(8,128)} async-done(((f32[64,3072]{1,0:T(8,128)}), f32[8,3072]{1,0:T(8,128)}) %reduce-scatter.4.cloned.1.call-update) | async-done | bytes 98320 | tf_op jit(solution)/shard_map/reduce_scatter | solution.py:47
  54.0 0.9 convert.8
  55.1 5.7 %fusion.57 = f32[8,8,1,512]{3,2,1,0:T(1,128)S(1)} fusion(bf16[8,8,512,128]{3,2,1,0:T(8,128)(2,1)} %param.28, bf16[8,8,128,1]{2,0,1,3:T(8,128)(2,1)S(1)} %fusion.59), kind=kOutput, calls=%fused_computation.69 | convolution fusion | flops 8388608 | bytes 8536064 | tf_op jit(solution)/shard_map/shd,shld->shl/dot_general | solution.py:62
  61.0 39.6 %reduce-window.6 = f32[8,8,4,128]{3,1,2,0:T(8,128)S(1)} reduce-window(f32[8,8,4,128]{3,1,2,0:T(8,128)S(1)} %fusion.35, f32[]{:T(128)} %constant.19.clone.1), window={size=1x1x1x128 pad=0_0x0_0x0_0x0_127}, to_apply=%region_3.0 | reduce-window | flops 4161536 | bytes 262148 | tf_op jit(solution)/shard_map/reduce-window
  101.3 4.7 %fusion.33 = f32[8,8,1,128]{3,2,1,0:T(1,128)S(1)} fusion(bf16[8,8,512,128]{3,2,1,0:T(8,128)(2,1)} %param.29, bf16[8,8,512,1]{2,1,0,3:T(8,128)(2,1)S(1)} %fusion.48), kind=kOutput, calls=%fused_computation.35 | convolution fusion | flops 8388608 | bytes 8486912 | tf_op jit(solution)/shard_map/shl,shld->shd/dot_general | solution.py:71
  106.7 8.4 %all-gather = bf16[32,2048]{1,0:T(8,128)(2,1)S(1)} all-gather(bf16[8,2048]{1,0:T(8,128)(2,1)S(1)} %convolution_convert_fusion.2), channel_id=2, replica_groups=mesh['ep'=8,'tp'=4] {'tp'}, dimensions={0}, use_global_device_ids=true | all-gather | bytes 163840 | tf_op jit(solution)/shard_map/all_gather | solution.py:74
  115.5 0.7 reshape.161
  116.2 3.4 %all-to-all-start.1 = ((bf16[8,4,2048]{2,1,0:T(4,128)(2,1)}), bf16[8,4,2048]{2,1,0:T(4,128)(2,1)S(1)}, u32[]{:S(2)}, u32[]{:S(2)}) async-start(bf16[8,4,2048]{2,1,0:T(4,128)(2,1)} %reshape.161), calls=%async_computation.2 | async-start | bytes 262144 | tf_op jit(solution)/shard_map/all_to_all | solution.py:105
  119.7 1.5 fusion.81
  122.0 0.7 fusion.52
  122.7 3.6 %all-to-all-done.1 = bf16[8,4,2048]{2,1,0:T(4,128)(2,1)S(1)} async-done(((bf16[8,4,2048]{2,1,0:T(4,128)(2,1)}), bf16[8,4,2048]{2,1,0:T(4,128)(2,1)S(1)}, u32[]{:S(2)}, u32[]{:S(2)}) %all-to-all-start.1) | async-done | bytes 131104 | tf_op jit(solution)/shard_map/all_to_all | solution.py:105
  126.3 2.3 %fusion.4 = f32[32,640]{1,0:T(8,128)S(1)} fusion(bf16[32,2048]{1,0:T(8,128)(2,1)S(1)} %reshape.162, bf16[1,2048,640]{2,1,0:T(8,128)(2,1)} %param.35), kind=kOutput, calls=%fused_computation.4 | convolution fusion | flops 83886080 | bytes 2834432 | tf_op jit(solution)/shard_map/dot_general | solution.py:107
  128.6 3.4 %fusion.6 = bf16[32,2048]{1,0:T(8,128)(2,1)} fusion(bf16[1,640,2048]{2,1,0:T(8,128)(2,1)S(1)} %copy-done, bf16[32,2048]{1,0:T(8,128)(2,1)S(1)} %reshape.162, bf16[1,2048,640]{2,1,0:T(8,128)(2,1)} %param.36, f32[32,640]{1,0:T(8,128)S(1)} %fusion.4), kind=kOutput, calls=%fused_computation.6 | convolution fusion | flops 167960576 | bytes 5586944 | tf_op jit(solution)/shard_map/dot_general | solution.py:110
  132.1 2.9 %convolution_convert_fusion.1 = bf16[8,2048]{1,0:T(8,128)(2,1)} fusion(bf16[256,2048]{1,0:T(8,128)(2,1)} %param.40, bf16[2048,256]{1,0:T(8,128)(2,1)} %param.39, f32[8,256]{1,0:T(8,128)S(1)} %fusion.81, bf16[8,2048]{1,0:T(8,128)(2,1)S(1)} %get-tuple-element.6, f32[2048]{0:T(1024)S(1)} %copy-done.3, f32[8]{0:T(128)S(1)} %add_rsqrt_fusion.2), kind=kOutput, calls=%fused_computation.8 | convolution fusion | flops 16871424 | bytes 2179104 | tf_op jit(solution)/shard_map/dot_general | solution.py:85
  135.0 19.4 %reduce-scatter.6.cloned.1.call-done = bf16[32,512]{1,0:T(8,128)(2,1)} async-done(((bf16[32,2048]{1,0:T(8,128)(2,1)}), bf16[32,512]{1,0:T(8,128)(2,1)}) %reduce-scatter.6.cloned.1.call-update) | async-done | bytes 32784 | tf_op jit(solution)/shard_map/reduce_scatter | solution.py:112
  154.4 1.4 reshape.163
  155.8 4.6 %all-to-all-start.2 = ((bf16[8,4,512]{2,1,0:T(4,128)(2,1)}), bf16[8,4,512]{2,1,0:T(4,128)(2,1)S(1)}, u32[]{:S(2)}, u32[]{:S(2)}) async-start(bf16[8,4,512]{2,1,0:T(4,128)(2,1)} %reshape.163), calls=%async_computation.4 | async-start | bytes 65536 | tf_op jit(solution)/shard_map/all_to_all | solution.py:119
  160.4 5.7 %all-to-all-done.2 = bf16[8,4,512]{2,1,0:T(4,128)(2,1)S(1)} async-done(((bf16[8,4,512]{2,1,0:T(4,128)(2,1)}), bf16[8,4,512]{2,1,0:T(4,128)(2,1)S(1)}, u32[]{:S(2)}, u32[]{:S(2)}) %all-to-all-start.2) | async-done | bytes 32800 | tf_op jit(solution)/shard_map/all_to_all | solution.py:119
  166.4 14.9 %reduce-scatter.8.cloned.1.call-done = bf16[8,512]{1,0:T(8,128)(2,1)} async-done(((bf16[8,2048]{1,0:T(8,128)(2,1)}), bf16[8,512]{1,0:T(8,128)(2,1)}) %reduce-scatter.8.cloned.1.call-update) | async-done | bytes 8208 | tf_op jit(solution)/shard_map/reduce_scatter | solution.py:115
  181.2 1.4 add_convert_fusion
  (59 shorter events, 4.1 us)
Async XLA Ops:
  7.2 121.4 %copy-start = (bf16[1,640,2048]{2,1,0:T(8,128)(2,1)S(1)}, bf16[1,640,2048]{2,1,0:T(8,128)(2,1)}, u32[]{:S(2)}) copy-start(bf16[1,640,2048]{2,1,0:T(8,128)(2,1)} %param.37) | copy-start | bytes 7864324
  7.2 16.5 %copy-start.6 = (s32[8,2]{0,1:T(2,128)S(1)}, s32[8,2]{0,1:T(2,128)}, u32[]{:S(2)}) copy-start(s32[8,2]{0,1:T(2,128)} %param.33) | copy-start | bytes 196
  7.2 17.2 %copy-start.8 = (s32[8]{0:T(128)S(1)}, s32[8]{0:T(128)}, u32[]{:S(2)}) copy-start(s32[8]{0:T(128)} %param.30) | copy-start | bytes 100
  7.2 47.8 %copy-start.7 = (f32[128]{0:T(128)S(1)}, f32[128]{0:T(128)}, u32[]{:S(2)}) copy-start(f32[128]{0:T(128)} %param.26) | copy-start | bytes 1540
  7.2 46.8 %reduce-scatter.4.cloned.1.call-start = ((), (), s32[]{:S(2)}) async-start(), calls=%async_computation.6 | async-start | bytes 884736 | tf_op jit(solution)/shard_map/reduce_scatter | solution.py:47
  55.1 5.7 %copy-start.5 = (f32[8]{0:T(128)S(1)}, f32[8]{0:T(128)}, u32[]{:S(2)}) copy-start(f32[8]{0:T(128)} %param.27) | copy-start | bytes 100
  101.3 4.8 %copy-start.1 = (bf16[1024,2048]{1,0:T(8,128)(2,1)S(1)}, bf16[1024,2048]{1,0:T(8,128)(2,1)}, u32[]{:S(2)}) copy-start(bf16[1024,2048]{1,0:T(8,128)(2,1)} %param.31) | copy-start | bytes 12582916
  106.0 9.1 %copy-start.2 = (bf16[8,2048]{1,0:T(8,128)(2,1)S(1)}, bf16[8,2048]{1,0:T(8,128)(2,1)}, u32[]{:S(2)}) copy-start(bf16[8,2048]{1,0:T(8,128)(2,1)} %param.21) | copy-start | bytes 98308
  106.0 9.3 %copy-start.3 = (f32[2048]{0:T(1024)S(1)}, f32[2048]{0:T(1024)}, u32[]{:S(2)}) copy-start(f32[2048]{0:T(1024)} %param.32) | copy-start | bytes 24580
  106.0 15.1 %copy-start.4 = (f32[2048]{0:T(1024)S(1)}, f32[2048]{0:T(1024)}, u32[]{:S(2)}) copy-start(f32[2048]{0:T(1024)} %param.41) | copy-start | bytes 24580
  116.2 10.1 %all-to-all-start.1 = ((bf16[8,4,2048]{2,1,0:T(4,128)(2,1)}), bf16[8,4,2048]{2,1,0:T(4,128)(2,1)S(1)}, u32[]{:S(2)}, u32[]{:S(2)}) async-start(bf16[8,4,2048]{2,1,0:T(4,128)(2,1)} %reshape.161), calls=%async_computation.2 | async-start | bytes 262144 | tf_op jit(solution)/shard_map/all_to_all | solution.py:105
  119.6 34.8 %reduce-scatter.6.cloned.1.call-start = ((), (), s32[]{:S(2)}) async-start(), calls=%async_computation.7 | async-start | bytes 163840 | tf_op jit(solution)/shard_map/reduce_scatter | solution.py:112
  128.6 37.6 %copy-start.9 = (f32[8,2]{0,1:T(2,128)S(1)}, f32[8,2]{0,1:T(2,128)}, u32[]{:S(2)}) copy-start(f32[8,2]{0,1:T(2,128)} %param.34) | copy-start | bytes 196
  132.0 49.2 %reduce-scatter.8.cloned.1.call-start = ((), (), s32[]{:S(2)}) async-start(), calls=%async_computation.8 | async-start | bytes 40960 | tf_op jit(solution)/shard_map/reduce_scatter | solution.py:115
  155.8 10.4 %all-to-all-start.2 = ((bf16[8,4,512]{2,1,0:T(4,128)(2,1)}), bf16[8,4,512]{2,1,0:T(4,128)(2,1)S(1)}, u32[]{:S(2)}, u32[]{:S(2)}) async-start(bf16[8,4,512]{2,1,0:T(4,128)(2,1)} %reshape.163), calls=%async_computation.4 | async-start | bytes 65536 | tf_op jit(solution)/shard_map/all_to_all | solution.py:119
Sparse Core Ops, SparseCore 0:
  23.8 30.1 reduce-scatter.3
  132.2 22.2 reduce-scatter.5
  157.2 24.0 reduce-scatter.7
